TPU v7x, 32 devices: a whole 2x2x4 slice. The times are simulated.
32 devices in a mesh: grp: 2 (over x), ep: 8 (over z, y), tp: 2 (over core).
Axes of the slice: x: 2, y: 2, z: 4, core: 2. Of those that a mesh axis runs over, the one named last changes fastest.
Arguments:
- tokens: bfloat16 [8192, 2048], P(('grp', 'ep', 'tp')), parts along dimension 0, may hold values from -6 to 6
- norm_gain: float32 [2048], replicated, may hold values from 0.1 to 1.9
- expert_ids: int32 [8192, 2], P(('grp', 'ep', 'tp')), parts along dimension 0, may hold values from 0 to 15, all different within a row; in each aligned block of 256 rows (0 to 255, 256 to 511, ...) at most 64 rows name the same one
- gate_values: float32 [8192, 2], P(('grp', 'ep', 'tp')), parts along dimension 0, may hold values from 0.2 to 2
- w_gate: bfloat16 [16, 2048, 512], P('ep', None, 'tp'), may hold values from -0.125 to 0.125
- w_up: bfloat16 [16, 2048, 512], P('ep', None, 'tp'), may hold values from -0.125 to 0.125
- w_down: bfloat16 [16, 512, 2048], P('ep', 'tp'), may hold values from -0.25 to 0.25
- s_gate: bfloat16 [2048, 512], P(None, 'tp'), may hold values from -0.125 to 0.125
- s_up: bfloat16 [2048, 512], P(None, 'tp'), may hold values from -0.125 to 0.125
- s_down: bfloat16 [512, 2048], P('tp'), may hold values from -0.25 to 0.25
Outputs:
- mixed: bfloat16 [8192, 2048], P(('grp', 'ep', 'tp')), parts along dimension 0
There are 2 independent parts, one for each index of `grp`. A program takes and returns all parts, laid end to end along the dimension named above; an argument that names none is the same for every part. Nothing has to cross between parts.
Inputs may be any that keep to these rules, and one draw needn't show every extreme that they name: `expert_ids`: each row names 2 different experts. Within the rows of one device no expert is named by more than 64 rows, a bound that some block reaches.
All inputs are finite; a program needn't handle non-finite values.
Results may differ from a plain program's by a relative error of at most 0.0068.
Values may be sent and summed in bfloat16 or wider, within the bound.
A program may use at most 128 MiB of HBM per device.

v0:
```python
import jax
import jax.numpy as jnp
from jax import lax
from jax.sharding import PartitionSpec as P


def swiglu_rows(rows, first_w, second_w):
    first = jnp.einsum("xecd,edf->xecf", rows, first_w, preferred_element_type=jnp.float32)
    second = jnp.einsum("xecd,edf->xecf", rows, second_w, preferred_element_type=jnp.float32)
    return (jax.nn.silu(first) * second).astype(jnp.bfloat16)


def shared_swiglu(rows, first_w, second_w):
    first = jnp.dot(rows, first_w, preferred_element_type=jnp.float32)
    second = jnp.dot(rows, second_w, preferred_element_type=jnp.float32)
    return (jax.nn.silu(first) * second).astype(jnp.bfloat16)


def body(tokens, norm_gain, expert_ids, gate_values, w_gate, w_up, w_down, s_gate, s_up, s_down):
    n_rows, width = tokens.shape
    topk = expert_ids.shape[1]
    ep_size = lax.axis_size("ep")
    local_exp = w_gate.shape[0]
    experts_n = local_exp * ep_size
    capacity = 2 * n_rows * topk // experts_n
    xf = tokens.astype(jnp.float32)
    scale = lax.rsqrt(jnp.mean(xf * xf, axis=-1, keepdims=True) + 1e-06)
    normed = (xf * scale * norm_gain).astype(jnp.bfloat16)
    s_hidden = shared_swiglu(lax.all_gather(normed, "tp", axis=0, tiled=True), s_gate, s_up)
    shared = lax.psum_scatter(
        jnp.dot(s_hidden, s_down, preferred_element_type=jnp.float32),
        "tp",
        scatter_dimension=0,
        tiled=True,
    )
    flat_e = expert_ids.reshape(-1)
    onehot = (flat_e[:, None] == jnp.arange(experts_n, dtype=jnp.int32)[None, :]).astype(jnp.int32)
    before = jnp.cumsum(onehot, axis=0) - onehot
    slot = jnp.sum(before * onehot, axis=1)
    position = flat_e * capacity + slot
    flat_tok = jnp.arange(flat_e.shape[0], dtype=jnp.int32) // topk
    slot_tok = jnp.full((experts_n * capacity,), n_rows, jnp.int32).at[position].set(flat_tok)
    padded = jnp.concatenate([normed, jnp.zeros((1, width), jnp.bfloat16)], axis=0)
    outgoing = padded[slot_tok].reshape(ep_size, local_exp, capacity, width)
    arrived = lax.all_to_all(outgoing, "ep", split_axis=0, concat_axis=0, tiled=True)
    full_gate, full_up = (
        lax.all_gather(w_gate, "tp", axis=2, tiled=True),
        lax.all_gather(w_up, "tp", axis=2, tiled=True),
    )
    full_down = lax.all_gather(w_down, "tp", axis=1, tiled=True)
    hidden = swiglu_rows(arrived, full_gate, full_up)
    results = jnp.einsum("xecf,efd->xecd", hidden, full_down, preferred_element_type=jnp.float32)
    returned = lax.all_to_all(
        results.astype(jnp.bfloat16), "ep", split_axis=0, concat_axis=0, tiled=True
    )
    picked = returned.reshape(experts_n * capacity, width)[position].reshape(n_rows, topk, width)
    routed = jnp.sum(gate_values[:, :, None] * picked.astype(jnp.float32), axis=1)
    return (shared + routed).astype(jnp.bfloat16)


def solution(mesh):
    return jax.shard_map(
        body,
        mesh=mesh,
        in_specs=(
            P(("grp", "ep", "tp"), None),
            P(),
            P(("grp", "ep", "tp"), None),
            P(("grp", "ep", "tp"), None),
            P("ep", None, "tp"),
            P("ep", None, "tp"),
            P("ep", "tp", None),
            P(None, "tp"),
            P(None, "tp"),
            P("tp", None),
        ),
        out_specs=P(("grp", "ep", "tp"), None),
        check_vma=False,
    )
```

profile of v0, /device:TPU:0, one launch (start us, length us, event | category | flops | bytes accessed | tf_op | source)
XLA Modules:
  0.0 272.1 jit_solution(9954740168588440158)
XLA Ops:
  6.5 1.6 fusion.10
  8.1 2.5 fusion.12
  10.7 0.0 all-gather.7.cloned.1.call-start
  10.8 0.7 all-gather.7.cloned.1.call-update
  11.5 0.7 all-gather.11.cloned.1.call-update
  12.2 0.1 copy.21
  12.3 0.1 eq.29
  12.5 0.1 eq.25
  12.6 1.2 reduce-window.6
  13.8 0.2 slice_reduce_fusion
  14.1 0.1 copy.20
  14.2 0.2 mul.70
  14.4 0.1 concatenate.3
  14.5 0.1 fusion.36
  14.6 2.4 scatter_custom_fusion
  17.1 6.0 %gather_fusion = bf16[1024,2048]{1,0:T(8,128)(2,1)} fusion(bf16[257,2048]{1,0:T(8,128)(2,1)S(1)} %concatenate.3, s32[1024]{0:T(1024)S(1)} %fusion.38), kind=kCustom, calls=%fused_computation | custom fusion | bytes 8392704 | tf_op jit(solution)/shard_map/gather | solution.py:44
  23.1 7.3 %all-to-all-start = ((bf16[8,2,64,2048]{3,2,1,0:T(8,128)(2,1)}), bf16[8,2,64,2048]{3,2,1,0:T(8,128)(2,1)}, u32[]{:S(2)}, u32[]{:S(2)}) async-start(bf16[8,2,64,2048]{3,2,1,0:T(8,128)(2,1)} %bitcast.72), calls=%async_computation.1 | async-start | bytes 8388608 | tf_op jit(solution)/shard_map/all_to_all | solution.py:45
  30.5 0.5 all-gather.9.cloned.1.call-update
  31.0 0.0 reduce-scatter.2.cloned.1.call-start
  31.1 3.7 %fusion.46 = f32[512,256]{1,0:T(8,128)} fusion(bf16[512,2048]{1,0:T(8,128)(2,1)} %all-gather.5.cloned.1.call-done, bf16[2048,256]{1,0:T(8,128)(2,1)} %param.17), kind=kOutput, calls=%fused_computation.62 | convolution fusion | flops 536870912 | bytes 3670016 | tf_op jit(solution)/shard_map/dot_general | solution.py:14
  34.8 5.8 %fusion.26 = f32[512,2048]{1,0:T(8,128)} fusion(bf16[256,2048]{1,0:T(8,128)(2,1)S(1)} %copy-done, bf16[512,2048]{1,0:T(8,128)(2,1)S(1)} %copy-done.3, bf16[2048,256]{1,0:T(8,128)(2,1)} %param.18, f32[512,256]{1,0:T(8,128)} %fusion.46), kind=kOutput, calls=%fused_computation.28 | convolution fusion | flops 1074528256 | bytes 8912896 | tf_op jit(solution)/shard_map/dot_general | solution.py:31
  40.7 83.0 %all-to-all-done = bf16[8,2,64,2048]{3,2,1,0:T(8,128)(2,1)} async-done(((bf16[8,2,64,2048]{3,2,1,0:T(8,128)(2,1)}), bf16[8,2,64,2048]{3,2,1,0:T(8,128)(2,1)}, u32[]{:S(2)}, u32[]{:S(2)}) %all-to-all-start) | async-done | bytes 4194336 | tf_op jit(solution)/shard_map/all_to_all | solution.py:45
  123.7 5.8 %fusion.4 = f32[2,8,64,512]{3,2,1,0:T(8,128)S(1)} fusion(bf16[2,2048,512]{2,1,0:T(8,128)(2,1)} %all-gather.7.cloned.1.call-done, bf16[8,2,64,2048]{3,2,1,0:T(8,128)(2,1)} %all-to-all-done), kind=kOutput, calls=%fused_computation.7 | convolution fusion | flops 2147483648 | bytes 10485760 | tf_op jit(solution)/shard_map/xecd,edf->xecf/dot_general | solution.py:8
  129.5 11.2 %convert_bitcast_fusion = bf16[8,2,64,2048]{3,2,0,1:T(8,128)(2,1)} fusion(bf16[2,512,2048]{2,1,0:T(8,128)(2,1)} %all-gather.11.cloned.1.call-done, f32[2,8,64,512]{3,2,1,0:T(8,128)S(1)} %fusion.4, bf16[2,2048,512]{2,1,0:T(8,128)(2,1)} %all-gather.9.cloned.1.call-done, bf16[8,2,64,2048]{3,2,1,0:T(8,128)(2,1)} %all-to-all-done), kind=kOutput, calls=%fused_computation.10 | convolution fusion | flops 4300210176 | bytes 18874368 | tf_op jit(solution)/shard_map/xecf,efd->xecd/dot_general | solution.py:52
  140.7 4.7 %copy.26 = bf16[8,2,64,2048]{3,2,1,0:T(8,128)(2,1)} copy(bf16[8,2,64,2048]{3,2,0,1:T(8,128)(2,1)} %convert_bitcast_fusion) | data formatting | bytes 8388608 | tf_op jit(solution)/shard_map/convert_element_type | solution.py:54
  145.5 4.9 %all-to-all-start.1 = ((bf16[8,2,64,2048]{3,2,1,0:T(8,128)(2,1)}), bf16[8,2,64,2048]{3,2,1,0:T(8,128)(2,1)}, u32[]{:S(2)}, u32[]{:S(2)}) async-start(bf16[8,2,64,2048]{3,2,1,0:T(8,128)(2,1)} %copy.26), calls=%async_computation.2 | async-start | bytes 8388608 | tf_op jit(solution)/shard_map/all_to_all | solution.py:53
  150.4 0.1 copy.19
  150.6 92.2 %all-to-all-done.1 = bf16[8,2,64,2048]{3,2,1,0:T(8,128)(2,1)} async-done(((bf16[8,2,64,2048]{3,2,1,0:T(8,128)(2,1)}), bf16[8,2,64,2048]{3,2,1,0:T(8,128)(2,1)}, u32[]{:S(2)}, u32[]{:S(2)}) %all-to-all-start.1) | async-done | bytes 4194336 | tf_op jit(solution)/shard_map/all_to_all | solution.py:53
  242.7 7.1 %gather_fusion.1 = bf16[512,2048]{1,0:T(8,128)(2,1)S(1)} fusion(bf16[1024,2048]{1,0:T(8,128)(2,1)} %bitcast.13, s32[1024]{0:T(1024)S(1)} %pad_clamp_fusion), kind=kCustom, calls=%fused_computation.1 | custom fusion | bytes 4196352 | tf_op jit(solution)/shard_map/gather | solution.py:56
  249.9 4.0 %reshape.68 = f32[256,2,2048]{2,1,0:T(2,128)} reshape(bf16[512,2048]{1,0:T(8,128)(2,1)S(1)} %gather_fusion.1) | data formatting | bytes 6291456 | tf_op jit(solution)/shard_map/convert_element_type | solution.py:57
  253.9 8.9 %multiply_reduce_fusion = f32[256,2048]{1,0:T(8,128)S(1)} fusion(f32[256,2,2048]{2,1,0:T(2,128)} %reshape.68, f32[256,2]{1,0:T(8,128)S(1)} %copy.19), kind=kLoop, calls=%fused_computation.9 | loop fusion | flops 1572864 | bytes 6293504 | tf_op jit(solution)/shard_map/reduce_sum | solution.py:57
  262.8 2.8 %add_convert_fusion = bf16[256,2048]{1,0:T(8,128)(2,1)} fusion(f32[256,2048]{1,0:T(8,128)} %reduce-scatter.2.cloned.1.call-done, f32[256,2048]{1,0:T(8,128)S(1)} %multiply_reduce_fusion), kind=kLoop, calls=%fused_computation.25 | loop fusion | flops 1048576 | bytes 5242880 | tf_op jit(solution)/shard_map/convert_element_type | solution.py:58
  (31 shorter events, 0.3 us)
Async XLA Ops:
  6.5 28.3 %copy-start = (bf16[256,2048]{1,0:T(8,128)(2,1)S(1)}, bf16[256,2048]{1,0:T(8,128)(2,1)}, u32[]{:S(2)}) copy-start(bf16[256,2048]{1,0:T(8,128)(2,1)} %param.19) | copy-start | bytes 3145732
  6.5 24.5 %all-gather.5.cloned.1.call-start = ((), (), s32[]{:S(2)}) async-start(), calls=%async_computation.3 | async-start | bytes 3145728 | tf_op jit(solution)/shard_map/all_gather | solution.py:29
  10.7 1.5 copy-start.4
  10.7 3.7 %copy-start.2 = (bf16[256,2048]{1,0:T(8,128)(2,1)S(1)}, bf16[256,2048]{1,0:T(8,128)(2,1)}, u32[]{:S(2)}) copy-start(bf16[256,2048]{1,0:T(8,128)(2,1)} %fusion.12) | copy-start | bytes 3145732
  10.7 30.0 %all-gather.7.cloned.1.call-start = ((), (), s32[]{:S(2)}) async-start(), calls=%async_computation.5 | async-start | bytes 6291456 | tf_op jit(solution)/shard_map/all_gather | solution.py:47
  11.5 118.1 %all-gather.11.cloned.1.call-start = ((), (), s32[]{:S(2)}) async-start(), calls=%async_computation.7 | async-start | bytes 6291456 | tf_op jit(solution)/shard_map/all_gather | solution.py:50
  23.1 100.6 %all-to-all-start = ((bf16[8,2,64,2048]{3,2,1,0:T(8,128)(2,1)}), bf16[8,2,64,2048]{3,2,1,0:T(8,128)(2,1)}, u32[]{:S(2)}, u32[]{:S(2)}) async-start(bf16[8,2,64,2048]{3,2,1,0:T(8,128)(2,1)} %bitcast.72), calls=%async_computation.1 | async-start | bytes 8388608 | tf_op jit(solution)/shard_map/all_to_all | solution.py:45
  30.4 99.1 %all-gather.9.cloned.1.call-start = ((), (), s32[]{:S(2)}) async-start(), calls=%async_computation.6 | async-start | bytes 6291456 | tf_op jit(solution)/shard_map/all_gather | solution.py:48
  31.0 231.8 %reduce-scatter.2.cloned.1.call-start = ((), (), s32[]{:S(2)}) async-start(), calls=%async_computation.4 | async-start | bytes 6291456 | tf_op jit(solution)/shard_map/reduce_scatter | solution.py:30
  31.1 3.7 %copy-start.3 = (bf16[512,2048]{1,0:T(8,128)(2,1)S(1)}, bf16[512,2048]{1,0:T(8,128)(2,1)}, u32[]{:S(2)}) copy-start(bf16[512,2048]{1,0:T(8,128)(2,1)} %all-gather.5.cloned.1.call-done) | copy-start | bytes 6291460
  145.5 4.9 %copy-start.5 = (f32[256,2]{0,1:T(2,128)S(1)}, f32[256,2]{0,1:T(2,128)}, u32[]{:S(2)}) copy-start(f32[256,2]{0,1:T(2,128)} %param.13) | copy-start | bytes 6148
  145.5 97.3 %all-to-all-start.1 = ((bf16[8,2,64,2048]{3,2,1,0:T(8,128)(2,1)}), bf16[8,2,64,2048]{3,2,1,0:T(8,128)(2,1)}, u32[]{:S(2)}, u32[]{:S(2)}) async-start(bf16[8,2,64,2048]{3,2,1,0:T(8,128)(2,1)} %copy.26), calls=%async_computation.2 | async-start | bytes 8388608 | tf_op jit(solution)/shard_map/all_to_all | solution.py:53
  253.9 11.7 %copy-start.1 = (bf16[256,2048]{1,0:T(8,128)(2,1)S(1)}, bf16[256,2048]{1,0:T(8,128)(2,1)}, u32[]{:S(2)}) copy-start(bf16[256,2048]{1,0:T(8,128)(2,1)} %param.19) | copy-start | bytes 3145732
Sparse Core Ops, SparseCore 0:
  10.8 13.2 all-gather.4
  25.7 13.9 all-gather.6
  41.2 14.8 all-gather.10
  57.5 13.9 all-gather.8
  73.6 13.2 reduce-scatter.1
where the time goes:
time: 273 us; the launch traced here: 272 us
  waiting for transfers between devices  177 us (65%)
  matrix products  26.6 us (10%)
  local copies, waits for them, and re-layouts  25.5 us (9%)
  other arithmetic  17.1 us (6%)
  between operations  13.3 us (5%)
  starting transfers between devices  12.4 us (5%)
    all_to_all x1, waiting for transfers between devices, body(): lax.all_to_all(results.astype(jnp.bfloat16), 'ep', split_axis=0, concat_a...  92.2 us
    all_to_all x1, waiting for transfers between devices, body(): lax.all_to_all(outgoing, 'ep', split_axis=0, concat_axis=0, tiled=True)  83 us
    dot_general x1, matrix products, body(): jnp.einsum('xecf,efd->xecd', hidden, full_down, preferred_element_type=jn...  11.2 us
    reduce_sum x1, other arithmetic, body(): jnp.sum(gate_values[:, :, None] * picked.astype(jnp.float32), axis=1)  8.86 us
    all_to_all x1, starting transfers between devices, body(): lax.all_to_all(outgoing, 'ep', split_axis=0, concat_axis=0, tiled=True)  7.31 us
    gather x1, local copies, waits for them, and re-layouts, body(): returned.reshape(experts_n * capacity, width)[position]  7.13 us
    gather x1, local copies, waits for them, and re-layouts, body(): outgoing = padded[slot_tok].reshape(ep_size, local_exp, capacity, width)  6.04 us
    dot_general x1, matrix products, body(): jnp.dot(s_hidden, s_down, preferred_element_type=jnp.float32)  5.85 us
  transfers between devices with their start and end apart: 7, of which 2 were waited for; matrix products, arithmetic and copies ran while one was open for 23% of the time, Pallas kernels for 0%

commit v1 on v0

--- a/solution.py
+++ b/solution.py
@@ -1,7 +1,376 @@
+import functools
+
 import jax
 import jax.numpy as jnp
 from jax import lax
+from jax.experimental import pallas as pl
+from jax.experimental.pallas import tpu as pltpu
 from jax.sharding import PartitionSpec as P
+
+MESH = pl.DeviceIdType.MESH
+CHUNKS = 4
+
+
+def line_shape(ep_size):
+    inner = 1
+    while (2 * inner) ** 2 <= ep_size:
+        inner *= 2
+    return ep_size // inner, inner
+
+
+def dot(a, b):
+    return jnp.dot(a, b, preferred_element_type=jnp.float32)
+
+
+def fused_kernel(
+    Z, Y, topk, cap,
+    normed, table, wg, wu, wd, sg, su, sd, out,
+    blk, tab, arr, sel, res, nres, part, recv, shared,
+    G, U, Dn, Gs, Us, Ds,
+    lsem, wloc, wsend, wrecv, zsend, zrecv, ysend, yrecv, rsend, rrecv, dsend, drecv,
+):
+    ep = lax.axis_index("ep")
+    tp = lax.axis_index("tp")
+    z = ep // Y
+    y = ep % Y
+    NCH, T, DC = normed.shape
+    E = wg.shape[0]
+    R = E * cap
+    other = 1 - tp
+
+    barrier = pltpu.get_barrier_semaphore()
+    pl.semaphore_signal(barrier, inc=1, device_id={"tp": other}, device_id_type=MESH)
+    for dz in (1, Z - 1):
+        pl.semaphore_signal(
+            barrier, inc=1, device_id={"ep": ((z + dz) % Z) * Y + y}, device_id_type=MESH
+        )
+    for d in range(1, Y):
+        pl.semaphore_signal(
+            barrier, inc=1, device_id={"ep": z * Y + (y + d) % Y}, device_id_type=MESH
+        )
+
+    own_blk = pltpu.make_async_copy(normed, blk.at[z], lsem.at[0])
+    own_tab = pltpu.make_async_copy(table, tab.at[z], lsem.at[1])
+    own_blk.start()
+    own_tab.start()
+    weights = ((sg, Gs), (su, Us), (sd, Ds), (wg, G), (wu, U), (wd, Dn))
+    local = [
+        pltpu.make_async_copy(src, dst.at[tp], wloc.at[i]) for i, (src, dst) in enumerate(weights)
+    ]
+    for copy in local:
+        copy.start()
+    own_tab.wait()
+    own_blk.wait()
+    pl.semaphore_wait(barrier, 3 + Y - 1)
+
+    def z_copy(t, c, way):
+        to = {"ep": (z - 1 + 2 * way) * Y + y}
+        src, dst = (tab.at[t], tab.at[t]) if c == NCH else (blk.at[t, c], blk.at[t, c])
+        return pltpu.make_async_remote_copy(
+            src_ref=src, dst_ref=dst, send_sem=zsend.at[way, t, c], recv_sem=zrecv.at[t, c],
+            device_id=to, device_id_type=MESH,
+        )
+
+    def has_next(way):
+        nxt = z - 1 + 2 * way
+        return (nxt >= 0) & (nxt < Z)
+
+    for c in (NCH, *range(NCH)):
+        for way in range(2):
+            @pl.when(has_next(way))
+            def _():
+                z_copy(z, c, way).start()
+
+    remote = [
+        pltpu.make_async_remote_copy(
+            src_ref=src, dst_ref=dst.at[tp], send_sem=wsend.at[i], recv_sem=wrecv.at[i],
+            device_id={"tp": other}, device_id_type=MESH,
+        )
+        for i, (src, dst) in enumerate(weights)
+    ]
+    for copy in remote:
+        copy.start()
+
+    row_ids = lax.broadcasted_iota(jnp.int32, (R, T), 0).astype(jnp.float32)
+
+    def spread(t, rank, weighted):
+        ids = row_ids + (rank * R).astype(jnp.float32)
+        total = jnp.zeros((R, T), jnp.float32)
+        for k in range(topk):
+            value = tab[t, topk + k : topk + k + 1, :] if weighted else jnp.ones((1, T), jnp.float32)
+            total = total + jnp.where(tab[t, k : k + 1, :] == ids, value, 0.0)
+        return total.astype(jnp.bfloat16)
+
+    def y_copy(t, d, c):
+        return pltpu.make_async_remote_copy(
+            src_ref=sel.at[t, d - 1, c], dst_ref=arr.at[t, c, y],
+            send_sem=ysend.at[t, d - 1, c], recv_sem=yrecv.at[t, y, c],
+            device_id={"ep": z * Y + (y + d) % Y}, device_id_type=MESH,
+        )
+
+    def y_arrive(t, d, c):
+        from_y = (y + d) % Y
+        return pltpu.make_async_remote_copy(
+            src_ref=sel.at[t, d - 1, c], dst_ref=arr.at[t, c, from_y],
+            send_sem=ysend.at[t, d - 1, c], recv_sem=yrecv.at[t, from_y, c],
+            device_id={"ep": z * Y + from_y}, device_id_type=MESH,
+        )
+
+    def r_copy(t, d, c):
+        to_y = (y + d) % Y
+        return pltpu.make_async_remote_copy(
+            src_ref=res.at[t, c, to_y], dst_ref=nres.at[t, c, y],
+            send_sem=rsend.at[t, d - 1, c], recv_sem=rrecv.at[t, y, c],
+            device_id={"ep": z * Y + to_y}, device_id_type=MESH,
+        )
+
+    def r_arrive(t, d, c):
+        from_y = (y + d) % Y
+        return pltpu.make_async_remote_copy(
+            src_ref=res.at[t, c, from_y], dst_ref=nres.at[t, c, from_y],
+            send_sem=rsend.at[t, d - 1, c], recv_sem=rrecv.at[t, from_y, c],
+            device_id={"ep": z * Y + from_y}, device_id_type=MESH,
+        )
+
+    def d_copy(t, way, c):
+        return pltpu.make_async_remote_copy(
+            src_ref=part.at[t, c], dst_ref=recv.at[t + way, c],
+            send_sem=dsend.at[t, c], recv_sem=drecv.at[t + way, c],
+            device_id={"ep": (z - 1 + 2 * way) * Y + y}, device_id_type=MESH,
+        )
+
+    def both(j, body):
+        @pl.loop(0, 2)
+        def _(way):
+            t = z + (2 * way - 1) * j
+
+            @pl.when((t >= 0) & (t < Z))
+            def _():
+                body(t, way)
+
+    def choose(t, c):
+        for d in range(Y):
+            picked = dot(spread(t, z * Y + (y + d) % Y, False), blk[t, c]).astype(jnp.bfloat16)
+            if d == 0:
+                arr[t, c, y] = picked
+            else:
+                sel[t, d - 1, c] = picked
+                y_copy(t, d, c).start()
+
+    def arrive(j, c):
+        def body(t, way):
+            if c == 0:
+                z_copy(t, NCH, 0).wait_recv()
+            z_copy(t, c, 0).wait_recv()
+            for onward in range(2):
+                @pl.when((way == 1 - onward) & has_next(onward))
+                def _():
+                    if c == 0:
+                        z_copy(t, NCH, onward).start()
+                    z_copy(t, c, onward).start()
+            choose(t, c)
+
+        both(j, body)
+
+    def hidden_of(rows, gate_ref, up_ref):
+        first = second = None
+        for c in range(NCH):
+            g = dot(rows[c], gate_ref[c * DC : (c + 1) * DC, :])
+            u = dot(rows[c], up_ref[c * DC : (c + 1) * DC, :])
+            first = g if first is None else first + g
+            second = u if second is None else second + u
+        return (first / (1.0 + jnp.exp(-first)) * second).astype(jnp.bfloat16)
+
+    def experts(t):
+        for d in range(1, Y):
+            for c in range(NCH):
+                y_arrive(t, d, c).wait_recv()
+
+        @pl.loop(0, E)
+        def _(e):
+            mine = pl.ds(pl.multiple_of(e * cap, cap), cap)
+            rows = [arr[t, c, :, mine, :].reshape(Y * cap, DC) for c in range(NCH)]
+            halves = [hidden_of(rows, G.at[h, e], U.at[h, e]) for h in range(2)]
+            for c in range(NCH):
+                cols = slice(c * DC, (c + 1) * DC)
+                o = dot(halves[0], Dn[0, e, :, cols]) + dot(halves[1], Dn[1, e, :, cols])
+                res[t, c, :, mine, :] = o.astype(jnp.bfloat16).reshape(Y, cap, DC)
+
+        for c in range(NCH):
+            for d in range(1, Y):
+                r_copy(t, d, c).start()
+
+    def merged(t, c):
+        total = None
+        for d in range(Y):
+            from_y = (y + d) % Y
+            if d:
+                r_arrive(t, d, c).wait_recv()
+            rows = res[t, c, y] if d == 0 else nres[t, c, from_y]
+            weight = spread(t, z * Y + from_y, True)
+            add = lax.dot_general(
+                weight, rows, (((0,), (0,)), ((), ())), preferred_element_type=jnp.float32
+            )
+            total = add if total is None else total + add
+        return total
+
+    def partial(t, way):
+        for c in range(NCH):
+            part[t, c] = merged(t, c).astype(jnp.bfloat16)
+
+    def pass_on(v):
+        for way in range(2):
+            t = v - z if way == 1 else 2 * (Z - 1) - z - v
+            ok = (t > z) & (t < Z) if way == 1 else (t >= 0) & (t < z)
+            upstream = z > 0 if way == 1 else z < Z - 1
+
+            @pl.when(ok)
+            def _():
+                for c in range(NCH):
+                    @pl.when(upstream)
+                    def _():
+                        d_copy(t, way, c).wait_recv()
+                        total = part[t, c].astype(jnp.float32) + recv[t + way, c].astype(jnp.float32)
+                        part[t, c] = total.astype(jnp.bfloat16)
+
+                    d_copy(t, way, c).start()
+
+    for c in range(NCH):
+        choose(z, c)
+    for copy in local[:3]:
+        copy.wait()
+    for copy in remote[:3]:
+        copy.wait_recv()
+    rows = [blk[z, c] for c in range(NCH)]
+    halves = [hidden_of(rows, Gs.at[h], Us.at[h]) for h in range(2)]
+    for c in range(NCH):
+        cols = slice(c * DC, (c + 1) * DC)
+        shared[c] = dot(halves[0], Ds[0, :, cols]) + dot(halves[1], Ds[1, :, cols])
+    for copy in local[3:]:
+        copy.wait()
+    for copy in remote[3:]:
+        copy.wait_recv()
+
+    last = Z - 1
+    for j in range(1, Z + 3):
+        for c in range(NCH):
+            if j <= last:
+                arrive(j, c)
+            if c == NCH // 2 - 1:
+                if j - 1 == 0:
+                    experts(z)
+                elif j - 1 <= last:
+                    both(j - 1, lambda t, way: experts(t))
+                if 1 <= j - 2 <= last:
+                    both(j - 2, partial)
+                    pass_on(j - 2)
+    for v in range(Z, 2 * Z - 2):
+        pass_on(v)
+
+    for c in range(NCH):
+        total = shared[c] + merged(z, c)
+        shared[c] = total
+        for way, there in ((0, z < Z - 1), (1, z > 0)):
+            @pl.when(there)
+            def _():
+                d_copy(z, way, c).wait_recv()
+                shared[c] += recv[z + way, c].astype(jnp.float32)
+
+        out[:, c * DC : (c + 1) * DC] = shared[c].astype(jnp.bfloat16)
+
+    for copy in remote:
+        copy.wait_send()
+    for way in range(2):
+        @pl.when(has_next(way))
+        def _():
+            @pl.loop(0, Z)
+            def _(t):
+                @pl.when((t <= z) if way == 1 else (t >= z))
+                def _():
+                    for c in range(NCH + 1):
+                        z_copy(t, c, way).wait_send()
+
+    @pl.loop(0, Z)
+    def _(t):
+        for c in range(NCH):
+            for d in range(1, Y):
+                y_copy(t, d, c).wait_send()
+                r_copy(t, d, c).wait_send()
+
+        @pl.when(t != z)
+        def _():
+            for c in range(NCH):
+                way = jnp.where(t > z, 1, 0)
+                d_copy(t, way, c).wait_send()
+
+
+def fused(tokens, norm_gain, expert_ids, gate_values, w_gate, w_up, w_down, s_gate, s_up, s_down):
+    T, D = tokens.shape
+    topk = expert_ids.shape[1]
+    ep_size = lax.axis_size("ep")
+    E, _, FH = w_gate.shape
+    SFH = s_gate.shape[1]
+    experts_n = E * ep_size
+    cap = 2 * T * topk // experts_n
+    Z, Y = line_shape(ep_size)
+    NCH = CHUNKS
+    DC = D // NCH
+    R = E * cap
+    bf, f32 = jnp.bfloat16, jnp.float32
+
+    xf = tokens.astype(f32)
+    scale = lax.rsqrt(jnp.mean(xf * xf, axis=-1, keepdims=True) + 1e-06)
+    normed = (xf * scale * norm_gain).astype(bf).reshape(T, NCH, DC).transpose(1, 0, 2)
+
+    onehot = expert_ids[:, :, None] == jnp.arange(experts_n, dtype=jnp.int32)
+    named = jnp.any(onehot, axis=1).astype(bf)
+    earlier = (jnp.arange(T)[:, None] > jnp.arange(T)[None, :]).astype(bf)
+    before = dot(earlier, named)
+    slot = jnp.sum(jnp.where(onehot, before[:, None, :], 0.0), axis=2)
+    position = expert_ids.astype(f32) * cap + slot
+    table = jnp.concatenate(
+        [position.T, gate_values.T, jnp.zeros((8 - 2 * topk, T), f32)], axis=0
+    )
+
+    vm, dma = pltpu.VMEM, pltpu.SemaphoreType.DMA
+    return pl.pallas_call(
+        functools.partial(fused_kernel, Z, Y, topk, cap),
+        out_shape=jax.ShapeDtypeStruct((T, D), bf),
+        in_specs=[pl.BlockSpec(memory_space=pl.ANY)] * 8,
+        out_specs=pl.BlockSpec(memory_space=pltpu.VMEM),
+        scratch_shapes=[
+            vm((Z, NCH, T, DC), bf),
+            vm((Z, 8, T), f32),
+            vm((Z, NCH, Y, R, DC), bf),
+            vm((Z, Y - 1, NCH, R, DC), bf),
+            vm((Z, NCH, Y, R, DC), bf),
+            vm((Z, NCH, Y, R, DC), bf),
+            vm((Z, NCH, T, DC), bf),
+            vm((Z + 1, NCH, T, DC), bf),
+            vm((NCH, T, DC), f32),
+            vm((2, E, D, FH), bf),
+            vm((2, E, D, FH), bf),
+            vm((2, E, FH, D), bf),
+            vm((2, D, SFH), bf),
+            vm((2, D, SFH), bf),
+            vm((2, SFH, D), bf),
+            dma((2,)),
+            dma((6,)),
+            dma((6,)),
+            dma((6,)),
+            dma((2, Z, NCH + 1)),
+            dma((Z, NCH + 1)),
+            dma((Z, Y - 1, NCH)),
+            dma((Z, Y, NCH)),
+            dma((Z, Y - 1, NCH)),
+            dma((Z, Y, NCH)),
+            dma((Z, NCH)),
+            dma((Z + 1, NCH)),
+        ],
+        compiler_params=pltpu.CompilerParams(
+            collective_id=0, has_side_effects=True, vmem_limit_bytes=63 * 1024 * 1024
+        ),
+    )(normed, table, w_gate, w_up, w_down, s_gate, s_up, s_down)
 
 
 def swiglu_rows(rows, first_w, second_w):
@@ -16,7 +385,7 @@
     return (jax.nn.silu(first) * second).astype(jnp.bfloat16)
 
 
-def body(tokens, norm_gain, expert_ids, gate_values, w_gate, w_up, w_down, s_gate, s_up, s_down):
+def exchanged(tokens, norm_gain, expert_ids, gate_values, w_gate, w_up, w_down, s_gate, s_up, s_down):
     n_rows, width = tokens.shape
     topk = expert_ids.shape[1]
     ep_size = lax.axis_size("ep")
@@ -58,6 +427,15 @@
     return (shared + routed).astype(jnp.bfloat16)
 
 
+def body(tokens, norm_gain, expert_ids, gate_values, w_gate, w_up, w_down, s_gate, s_up, s_down):
+    args = (tokens, norm_gain, expert_ids, gate_values, w_gate, w_up, w_down, s_gate, s_up, s_down)
+    local_exp = w_gate.shape[0]
+    cap = 2 * tokens.shape[0] * expert_ids.shape[1] // (local_exp * lax.axis_size("ep"))
+    if cap % 16 == 0 and lax.axis_size("tp") == 2:
+        return fused(*args)
+    return exchanged(*args)
+
+
 def solution(mesh):
     return jax.shard_map(
         body,

time: 273 us -> 178 us (0.65)
  waiting for transfers between devices: 177 us -> 0 us
  Pallas kernels: 0 us -> 168 us
  matrix products: 26.6 us -> 0.16 us
  local copies, waits for them, and re-layouts: 25.5 us -> 5.18 us
  between operations: 13.3 us -> 0.03 us
  other arithmetic: 17.1 us -> 4.11 us
  starting transfers between devices: 12.4 us -> 0 us
    all_to_all x2 -> x0, waiting for transfers between devices: 175 us -> none  [the longest x1 92.2 us: body(): lax.all_to_all(results.astype(jnp.bfloat16), 'ep', split_axis=0, concat_a...]
    pallas_call x0 -> x1, Pallas kernels: none -> 168 us  [fused(): pl.pallas_call(functools.partial(fused_kernel, Z, Y, topk, cap), out_shap...]
    dot_general x4 -> x1, matrix products: 26.6 us -> 0.16 us  [dot(): return jnp.dot(a, b, preferred_element_type=jnp.float32)]
    gather x2 -> x0, local copies, waits for them, and re-layouts: 13.2 us -> none  [the longest x1 7.13 us: body(): returned.reshape(experts_n * capacity, width)[position]]
    all_to_all x2 -> x0, starting transfers between devices: 12.2 us -> none  [the longest x1 7.31 us: body(): lax.all_to_all(outgoing, 'ep', split_axis=0, concat_axis=0, tiled=True)]
    reduce_sum x3 -> x2, other arithmetic: 10.5 us -> 1.04 us  [the longest x1 0.73 us: fused(): slot = jnp.sum(jnp.where(onehot, before[:, None, :], 0.0), axis=2)]
    convert_element_type x2 -> x0, local copies, waits for them, and re-layouts: 8.72 us -> none  [the longest x1 4.75 us: body(): results.astype(jnp.bfloat16)]
    convert_element_type x3 -> x1, other arithmetic: 5.32 us -> 0.34 us  [fused(): (xf * scale * norm_gain).astype(bf).reshape(T, NCH, DC).transpose(1, 0, 2)]
  transfers between devices with their start and end apart: 7 -> 0, of which waited for: 2 -> 0; matrix products, arithmetic and copies ran while one was open for 23% -> 0% of each run, Pallas kernels for 0% -> 0%
where the time goes in v1:
time: 178 us
  Pallas kernels  168 us (94%)
  local copies, waits for them, and re-layouts  5.18 us (3%)
  other arithmetic  4.11 us (2%)
    pallas_call x1, Pallas kernels, fused(): pl.pallas_call(functools.partial(fused_kernel, Z, Y, topk, cap), out_shap...  168 us
    unnamed x4, local copies, waits for them, and re-layouts  3.78 us

profile of v1, /device:TPU:0, one launch (start us, length us, event | category | flops | bytes accessed | tf_op | source)
XLA Modules:
  0.0 177.8 jit_solution(14625980389662873361)
XLA Ops:
  0.0 0.0 copy-start
  0.0 0.1 pad.2.clone
  0.1 0.7 fusion.4
  0.8 0.2 fusion.3
  0.9 0.7 select_reduce_fusion
  1.7 0.7 add_bitcast_fusion
  2.4 1.3 maximum_maximum_fusion.table
  3.7 1.5 copy.17
  5.2 0.3 fusion
  5.5 0.0 copy-done
  5.5 0.3 fusion.2
  5.8 1.3 copy.18
  7.2 168.3 %shard_map.100 = bf16[256,2048]{1,0:T(8,128)(2,1)} custom-call(bf16[4,256,512]{2,1,0:T(8,128)(2,1)} %bitcast.6, f32[8,256]{1,0:T(8,128)} %maximum_maximum_fusion.table, bf16[2,2048,256]{2,1,0:T(8,128)(2,1)} %wg.1, bf16[2,2048,256]{2,1,0:T(8,128)(2,1)} %wu.1, bf16[2,256,2048]{2,1,0:T(8,128)(2,1)} %wd.1, bf16[2048,256]{1,0:T(8,128)(2,1)} %sg.1, ...), custom_call_target="tpu_custom_call" | custom-call | tf_op jit(solution)/shard_map/pallas_call | solution.py:336
  175.5 2.3 %copy.20 = bf16[256,2048]{1,0:T(8,128)(2,1)} copy(bf16[256,2048]{1,0:T(8,128)(2,1)} %shard_map.100) | data formatting | bytes 2097152
  (2 shorter events, 0.0 us)
Async XLA Ops:
  0.0 5.5 %copy-start = (f32[2048]{0:T(1024)S(1)}, f32[2048]{0:T(1024)}, u32[]{:S(2)}) copy-start(f32[2048]{0:T(1024)} %param.11) | copy-start | bytes 24580

commit v2 on v1

--- a/solution.py
+++ b/solution.py
@@ -24,8 +24,8 @@
 
 def fused_kernel(
     Z, Y, topk, cap,
-    normed, table, wg, wu, wd, sg, su, sd, out,
-    blk, tab, arr, sel, res, nres, part, recv, shared,
+    tokens, gain, ids, gates, wg, wu, wd, sg, su, sd, out,
+    tok, blk, tab, arr, sel, res, nres, part, recv, shared,
     G, U, Dn, Gs, Us, Ds,
     lsem, wloc, wsend, wrecv, zsend, zrecv, ysend, yrecv, rsend, rrecv, dsend, drecv,
 ):
@@ -33,7 +33,9 @@
     tp = lax.axis_index("tp")
     z = ep // Y
     y = ep % Y
-    NCH, T, DC = normed.shape
+    T, D = tokens.shape
+    NCH = CHUNKS
+    DC = D // NCH
     E = wg.shape[0]
     R = E * cap
     other = 1 - tp
@@ -49,18 +51,41 @@
             barrier, inc=1, device_id={"ep": z * Y + (y + d) % Y}, device_id_type=MESH
         )
 
-    own_blk = pltpu.make_async_copy(normed, blk.at[z], lsem.at[0])
-    own_tab = pltpu.make_async_copy(table, tab.at[z], lsem.at[1])
-    own_blk.start()
-    own_tab.start()
+    own = pltpu.make_async_copy(tokens, tok, lsem.at[0])
+    own.start()
     weights = ((sg, Gs), (su, Us), (sd, Ds), (wg, G), (wu, U), (wd, Dn))
     local = [
         pltpu.make_async_copy(src, dst.at[tp], wloc.at[i]) for i, (src, dst) in enumerate(weights)
     ]
     for copy in local:
         copy.start()
-    own_tab.wait()
-    own_blk.wait()
+
+    experts_n = E * Z * Y
+    expert = lax.broadcasted_iota(jnp.int32, (experts_n, T), 0).astype(jnp.float32)
+    named = ids[...].astype(jnp.float32)
+    chosen = [(named[k : k + 1, :] == expert).astype(jnp.float32) for k in range(topk)]
+    earlier = lax.broadcasted_iota(jnp.int32, (T, T), 0) < lax.broadcasted_iota(jnp.int32, (T, T), 1)
+    before = dot(
+        sum(chosen).astype(jnp.bfloat16), jnp.where(earlier, 1.0, 0.0).astype(jnp.bfloat16)
+    )
+    for k in range(topk):
+        slot = jnp.sum(before * chosen[k], axis=0, keepdims=True)
+        tab[z, k : k + 1, :] = named[k : k + 1, :] * cap + slot
+        tab[z, topk + k : topk + k + 1, :] = gates[k : k + 1, :]
+    tab[z, 2 * topk :, :] = jnp.zeros((8 - 2 * topk, T), jnp.float32)
+
+    own.wait()
+    step = 16
+
+    @pl.loop(0, T // step)
+    def _(i):
+        some = pl.ds(pl.multiple_of(i * step, step), step)
+        x = tok[some, :].astype(jnp.float32)
+        scale = lax.rsqrt(jnp.mean(x * x, axis=-1, keepdims=True) + 1e-06)
+        x = (x * scale * gain[...]).astype(jnp.bfloat16)
+        for c in range(NCH):
+            blk[z, c, some, :] = x[:, c * DC : (c + 1) * DC]
+
     pl.semaphore_wait(barrier, 3 + Y - 1)
 
     def z_copy(t, c, way):
@@ -214,11 +239,13 @@
             total = add if total is None else total + add
         return total
 
-    def partial(t, way):
-        for c in range(NCH):
+    def partial(j, c):
+        def body(t, way):
             part[t, c] = merged(t, c).astype(jnp.bfloat16)
 
-    def pass_on(v):
+        both(j, body)
+
+    def pass_on(v, c):
         for way in range(2):
             t = v - z if way == 1 else 2 * (Z - 1) - z - v
             ok = (t > z) & (t < Z) if way == 1 else (t >= 0) & (t < z)
@@ -226,14 +253,23 @@
 
             @pl.when(ok)
             def _():
-                for c in range(NCH):
-                    @pl.when(upstream)
-                    def _():
-                        d_copy(t, way, c).wait_recv()
-                        total = part[t, c].astype(jnp.float32) + recv[t + way, c].astype(jnp.float32)
-                        part[t, c] = total.astype(jnp.bfloat16)
-
-                    d_copy(t, way, c).start()
+                @pl.when(upstream)
+                def _():
+                    d_copy(t, way, c).wait_recv()
+                    total = part[t, c].astype(jnp.float32) + recv[t + way, c].astype(jnp.float32)
+                    part[t, c] = total.astype(jnp.bfloat16)
+
+                d_copy(t, way, c).start()
+
+    def finish(c):
+        shared[c] += merged(z, c)
+        for way, there in ((0, z < Z - 1), (1, z > 0)):
+            @pl.when(there)
+            def _():
+                d_copy(z, way, c).wait_recv()
+                shared[c] += recv[z + way, c].astype(jnp.float32)
+
+        out[:, c * DC : (c + 1) * DC] = shared[c].astype(jnp.bfloat16)
 
     for c in range(NCH):
         choose(z, c)
@@ -252,31 +288,24 @@
         copy.wait_recv()
 
     last = Z - 1
-    for j in range(1, Z + 3):
+    for j in range(1, Z):
         for c in range(NCH):
-            if j <= last:
-                arrive(j, c)
-            if c == NCH // 2 - 1:
-                if j - 1 == 0:
-                    experts(z)
-                elif j - 1 <= last:
-                    both(j - 1, lambda t, way: experts(t))
-                if 1 <= j - 2 <= last:
-                    both(j - 2, partial)
-                    pass_on(j - 2)
-    for v in range(Z, 2 * Z - 2):
-        pass_on(v)
-
-    for c in range(NCH):
-        total = shared[c] + merged(z, c)
-        shared[c] = total
-        for way, there in ((0, z < Z - 1), (1, z > 0)):
-            @pl.when(there)
-            def _():
-                d_copy(z, way, c).wait_recv()
-                shared[c] += recv[z + way, c].astype(jnp.float32)
-
-        out[:, c * DC : (c + 1) * DC] = shared[c].astype(jnp.bfloat16)
+            arrive(j, c)
+            if j == 1 and c == NCH // 2 - 1:
+                experts(z)
+        if j > 1:
+            for c in range(NCH):
+                partial(j - 1, c)
+                pass_on(j - 1, c)
+        both(j, lambda t, way: experts(t))
+
+    for _, v, c in sorted((v + c, v, c) for v in range(last, 2 * Z - 1) for c in range(NCH)):
+        if v == last:
+            partial(last, c)
+        if v < 2 * last:
+            pass_on(v, c)
+        else:
+            finish(c)
 
     for copy in remote:
         copy.wait_send()
@@ -310,35 +339,27 @@
     ep_size = lax.axis_size("ep")
     E, _, FH = w_gate.shape
     SFH = s_gate.shape[1]
-    experts_n = E * ep_size
-    cap = 2 * T * topk // experts_n
+    cap = 2 * T * topk // (E * ep_size)
     Z, Y = line_shape(ep_size)
     NCH = CHUNKS
     DC = D // NCH
     R = E * cap
     bf, f32 = jnp.bfloat16, jnp.float32
 
-    xf = tokens.astype(f32)
-    scale = lax.rsqrt(jnp.mean(xf * xf, axis=-1, keepdims=True) + 1e-06)
-    normed = (xf * scale * norm_gain).astype(bf).reshape(T, NCH, DC).transpose(1, 0, 2)
-
-    onehot = expert_ids[:, :, None] == jnp.arange(experts_n, dtype=jnp.int32)
-    named = jnp.any(onehot, axis=1).astype(bf)
-    earlier = (jnp.arange(T)[:, None] > jnp.arange(T)[None, :]).astype(bf)
-    before = dot(earlier, named)
-    slot = jnp.sum(jnp.where(onehot, before[:, None, :], 0.0), axis=2)
-    position = expert_ids.astype(f32) * cap + slot
-    table = jnp.concatenate(
-        [position.T, gate_values.T, jnp.zeros((8 - 2 * topk, T), f32)], axis=0
-    )
-
     vm, dma = pltpu.VMEM, pltpu.SemaphoreType.DMA
     return pl.pallas_call(
         functools.partial(fused_kernel, Z, Y, topk, cap),
         out_shape=jax.ShapeDtypeStruct((T, D), bf),
-        in_specs=[pl.BlockSpec(memory_space=pl.ANY)] * 8,
+        in_specs=[
+            pl.BlockSpec(memory_space=pl.ANY),
+            pl.BlockSpec(memory_space=pltpu.VMEM),
+            pl.BlockSpec(memory_space=pltpu.VMEM),
+            pl.BlockSpec(memory_space=pltpu.VMEM),
+        ]
+        + [pl.BlockSpec(memory_space=pl.ANY)] * 6,
         out_specs=pl.BlockSpec(memory_space=pltpu.VMEM),
         scratch_shapes=[
+            vm((T, D), bf),
             vm((Z, NCH, T, DC), bf),
             vm((Z, 8, T), f32),
             vm((Z, NCH, Y, R, DC), bf),
@@ -354,7 +375,7 @@
             vm((2, D, SFH), bf),
             vm((2, D, SFH), bf),
             vm((2, SFH, D), bf),
-            dma((2,)),
+            dma((1,)),
             dma((6,)),
             dma((6,)),
             dma((6,)),
@@ -370,7 +391,7 @@
         compiler_params=pltpu.CompilerParams(
             collective_id=0, has_side_effects=True, vmem_limit_bytes=63 * 1024 * 1024
         ),
-    )(normed, table, w_gate, w_up, w_down, s_gate, s_up, s_down)
+    )(tokens, norm_gain.reshape(1, D), expert_ids.T, gate_values.T, w_gate, w_up, w_down, s_gate, s_up, s_down)
 
 
 def swiglu_rows(rows, first_w, second_w):

time: 178 us -> 169 us (0.949)
  other arithmetic: 4.11 us -> 0 us
  local copies, waits for them, and re-layouts: 5.18 us -> 2.3 us
  Pallas kernels: 168 us -> 166 us
    pallas_call x1, Pallas kernels: 168 us -> 166 us  [fused(): pl.pallas_call(functools.partial(fused_kernel, Z, Y, topk, cap), out_shap...]
    unnamed x4 -> x1, local copies, waits for them, and re-layouts: 3.78 us -> 2.3 us
where the time goes in v2:
time: 169 us
  Pallas kernels  166 us (98%)
  local copies, waits for them, and re-layouts  2.3 us (1%)
    pallas_call x1, Pallas kernels, fused(): pl.pallas_call(functools.partial(fused_kernel, Z, Y, topk, cap), out_shap...  166 us

profile of v2, /device:TPU:0, one launch (start us, length us, event | category | flops | bytes accessed | tf_op | source)
XLA Modules:
  0.0 168.6 jit_solution(1081641043100650797)
XLA Ops:
  0.0 166.2 %shard_map.100 = bf16[256,2048]{1,0:T(8,128)(2,1)} custom-call(bf16[256,2048]{1,0:T(8,128)(2,1)} %tokens.1, f32[1,2048]{1,0:T(1,128)} %bitcast.3, s32[2,256]{1,0:T(2,128)} %bitcast.4, f32[2,256]{1,0:T(2,128)} %bitcast.5, bf16[2,2048,256]{2,1,0:T(8,128)(2,1)} %wg.1, bf16[2,2048,256]{2,1,0:T(8,128)(2,1)} %wu.1, bf16[2,256,2048]{2,1,0:T(8,128)(2,1)} %wd.1, ...), custom_call_target="tpu_custom_call" | custom-call | tf_op jit(solution)/shard_map/pallas_call | solution.py:350
  166.2 2.3 %copy.12 = bf16[256,2048]{1,0:T(8,128)(2,1)} copy(bf16[256,2048]{1,0:T(8,128)(2,1)} %shard_map.100) | data formatting | bytes 2097152
